TPU v7x, 32 devices: a whole 2x2x4 slice. The times are simulated.
32 devices in a mesh: sp: 4 (over z), fs: 4 (over y, x), tp: 2 (over core).
Axes of the slice: x: 2, y: 2, z: 4, core: 2. Of those that a mesh axis runs over, the one named last changes fastest.
Arguments:
- tokens: bfloat16 [8192, 2048], P(('fs', 'sp')), parts along dimension 0, may hold values from -6 to 6
- norm_gain: float32 [2048], replicated, may hold values from 0.1 to 1.9
- state_gate: bfloat16 [2048, 1024], P('sp', 'tp'), may hold values from -0.125 to 0.125
- state_value: bfloat16 [2048, 1024], P('sp', 'tp'), may hold values from -0.125 to 0.125
- state_keys: bfloat16 [2048, 1024], P('sp', 'tp'), may hold values from -0.125 to 0.125
- state_query: bfloat16 [2048, 1024], P('sp', 'tp'), may hold values from -0.125 to 0.125
- state_step: bfloat16 [2048, 16], replicated, may hold values from -0.125 to 0.125
- state_rate: float32 [16], P('tp'), may hold values from 0 to 1, as said below
- state_jumps: float32 [8192, 16], P(('fs', 'sp'), 'tp'), parts along dimension 0, may hold values from -3 to 0
- state_gain: float32 [1024], P('tp'), may hold values from 0.1 to 1.9
- filter_value: bfloat16 [5, 1024], P(None, 'tp'), may hold values from -2.5 to 2.5
- filter_keys: bfloat16 [5, 1024], P(None, 'tp'), may hold values from -2.5 to 2.5
- filter_query: bfloat16 [5, 1024], P(None, 'tp'), may hold values from -2.5 to 2.5
- window_query: bfloat16 [2048, 2048], P('sp', 'tp'), may hold values from -64 to 64
- window_keys: bfloat16 [2048, 1024], P('sp', 'tp'), may hold values from -1 to 1
- window_values: bfloat16 [2048, 1024], P('sp', 'tp'), may hold values from -0.125 to 0.125
- window_sink: float32 [16], P('tp'), may hold values from 2.5 to 5.5
- state_output: bfloat16 [1024, 2048], P('tp', 'sp'), may hold values from -0.1875 to 0.1875
- window_output: bfloat16 [2048, 2048], P('tp', 'sp'), may hold values from -2 to 2
Outputs:
- mixed: bfloat16 [8192, 2048], P(('fs', 'sp', 'tp')), parts along dimension 0
There are 4 independent parts, one for each index of `fs`. A program takes and returns all parts, laid end to end along the dimension named above; an argument that names none is the same for every part. Nothing has to cross between parts.
Inputs may be any that keep to these rules, and one draw needn't show every extreme that they name: `state_rate`: a positive rate for each head.
All inputs are finite; a program needn't handle non-finite values.
Results may differ from a plain program's by a relative error of at most 0.015.
The roundings to bfloat16 on the way count: a program that leaves them out, or rounds other values in their place, can miss the bound.
Values may be sent and summed in bfloat16 or wider, within the bound.
A program may use at most 64 MiB of HBM per device.

v0:
```python
import jax
import jax.numpy as jnp
from jax import lax
from jax.sharding import PartitionSpec as P

STATE_SIZE = 128
HEAD_DIM = 128
WINDOW = 128
BLOCK = 128
GRID_WIDTH = 64


def extended(cells, sides, width):
    for axis, dim in sides:
        count = lax.axis_size(axis)
        ends = count - 1
        head = lax.slice_in_dim(cells, 0, width, axis=dim)
        tail = lax.slice_in_dim(cells, cells.shape[dim] - width, cells.shape[dim], axis=dim)
        cells = jnp.concatenate(
            [
                lax.ppermute(tail, axis, [(i, (i + 1) % count) for i in range(ends)]),
                cells,
                lax.ppermute(head, axis, [((i + 1) % count, i) for i in range(ends)]),
            ],
            axis=dim,
        )
    return cells


def rotate_grid(vectors, positions, grid_width):
    head_dim = vectors.shape[-1]
    quarter = head_dim // 4
    half_dim = head_dim // 2
    inverse = 10000.0 ** (-jnp.arange(quarter, dtype=jnp.float32) / quarter)
    grid_row = (positions // grid_width).astype(jnp.float32)
    grid_col = (positions % grid_width).astype(jnp.float32)
    angle_row = grid_row[:, None] * inverse[None, :]
    angle_col = grid_col[:, None] * inverse[None, :]
    angles = jnp.concatenate([angle_row, angle_row, angle_col, angle_col], axis=-1)[:, None, :]
    first_half = vectors[..., :half_dim]
    second = vectors[..., half_dim:]
    turned = jnp.concatenate(
        [
            -first_half[..., quarter:],
            first_half[..., :quarter],
            -second[..., quarter:],
            second[..., :quarter],
        ],
        axis=-1,
    )
    return (
        vectors.astype(jnp.float32) * jnp.cos(angles) + turned.astype(jnp.float32) * jnp.sin(angles)
    ).astype(jnp.bfloat16)


def window_attend(query_rows, keys_pad, values_pad, sink_logits, key_start, total_len, window):
    row_count, query_heads, head_dim = query_rows.shape
    kv_heads = keys_pad.shape[1]
    group_size = query_heads // kv_heads
    block_count = row_count // window
    query_blocks = query_rows.reshape(block_count, window, kv_heads, group_size, head_dim)
    key_split = keys_pad.reshape(block_count + 2, window, kv_heads, head_dim)
    value_split = values_pad.reshape(block_count + 2, window, kv_heads, head_dim)
    key_band = jnp.concatenate([key_split[:-2], key_split[1:-1], key_split[2:]], axis=1)
    value_band = jnp.concatenate([value_split[:-2], value_split[1:-1], value_split[2:]], axis=1)
    scores = jnp.einsum(
        "kihgd,kjhd->khgij", query_blocks, key_band, preferred_element_type=jnp.float32
    ) * head_dim ** (-0.5)
    query_pos = jnp.arange(window)[:, None]
    band_pos = jnp.arange(3 * window)[None, :]
    within = jnp.abs(band_pos - window - query_pos) <= window
    key_pos = (
        key_start + jnp.arange(block_count)[:, None] * window + jnp.arange(3 * window)[None, :]
    )
    inside = (key_pos >= 0) & (key_pos < total_len)
    valid_pair = (within[None] & inside[:, None, :])[:, None, None]
    sink_logit = sink_logits.reshape(kv_heads, group_size)[None, :, :, None, None]
    masked = jnp.where(valid_pair, scores, -1e30)
    ceiling = jnp.maximum(jnp.max(masked, axis=-1, keepdims=True), sink_logit)
    weights = jnp.where(valid_pair, jnp.exp(masked - ceiling), 0.0)
    denominator = jnp.exp(sink_logit - ceiling) + jnp.sum(weights, axis=-1, keepdims=True)
    weights_bf = (weights / denominator).astype(jnp.bfloat16)
    mixed_rows = jnp.einsum(
        "khgij,kjhd->kihgd", weights_bf, value_band, preferred_element_type=jnp.float32
    )
    return mixed_rows.reshape(row_count, query_heads * head_dim).astype(jnp.bfloat16)


def block_terms(query_rows, key_rows, value_rows, log_rows, block_len):
    row_count, group_count, state_size = query_rows.shape
    head_ratio, head_dim = (value_rows.shape[2], value_rows.shape[3])
    block_count = row_count // block_len
    query_blocks = query_rows.reshape(block_count, block_len, group_count, state_size)
    key_blocks = key_rows.reshape(block_count, block_len, group_count, state_size)
    value_blocks = value_rows.reshape(block_count, block_len, group_count, head_ratio, head_dim)
    decay_cum = jnp.cumsum(
        log_rows.reshape(block_count, block_len, group_count, head_ratio), axis=1
    )
    decay_total = decay_cum[:, -1]
    gram_block = jnp.einsum(
        "kign,kjgn->kgij", query_blocks, key_blocks, preferred_element_type=jnp.float32
    )
    cum_heads = jnp.moveaxis(decay_cum, 1, 3)
    distance = jnp.abs(cum_heads[..., :, None] - cum_heads[..., None, :])
    pair_weight = (gram_block[:, :, None] * jnp.exp(-distance)).astype(jnp.bfloat16)
    near_terms = jnp.einsum(
        "kgrij,kjgrp->kigrp", pair_weight, value_blocks, preferred_element_type=jnp.float32
    )
    keys_after = (
        key_blocks[:, :, :, None, :] * jnp.exp(decay_total[:, None] - decay_cum)[..., None]
    ).astype(jnp.bfloat16)
    keys_before = (key_blocks[:, :, :, None, :] * jnp.exp(decay_cum)[..., None]).astype(
        jnp.bfloat16
    )
    state_after = jnp.einsum(
        "kjgrn,kjgrp->kgrnp", keys_after, value_blocks, preferred_element_type=jnp.float32
    )
    state_before = jnp.einsum(
        "kjgrn,kjgrp->kgrnp", keys_before, value_blocks, preferred_element_type=jnp.float32
    )
    before = jnp.cumsum(decay_total, axis=0) - decay_total
    overall = jnp.sum(decay_total, axis=0)
    after_sum = overall[None] - before - decay_total
    block_order = jnp.arange(block_count)
    earlier_mask = (block_order[None, :] < block_order[:, None])[:, :, None, None]
    later_mask = (block_order[None, :] > block_order[:, None])[:, :, None, None]
    gap_fwd = before[:, None] - before[None, :] - decay_total[None, :]
    gap_bwd = before[None, :] - before[:, None] - decay_total[:, None]
    weight_fwd = jnp.where(earlier_mask, jnp.exp(jnp.minimum(gap_fwd, 0.0)), 0.0)
    weight_bwd = jnp.where(later_mask, jnp.exp(jnp.minimum(gap_bwd, 0.0)), 0.0)
    carried_fwd = jnp.einsum(
        "abgr,bgrnp->agrnp", weight_fwd, state_after, precision=lax.Precision.HIGHEST
    )
    carried_bwd = jnp.einsum(
        "abgr,bgrnp->agrnp", weight_bwd, state_before, precision=lax.Precision.HIGHEST
    )
    summary_fwd = jnp.einsum(
        "agr,agrnp->grnp", jnp.exp(after_sum), state_after, precision=lax.Precision.HIGHEST
    )
    summary_bwd = jnp.einsum(
        "agr,agrnp->grnp", jnp.exp(before), state_before, precision=lax.Precision.HIGHEST
    )
    pieces = (
        near_terms,
        carried_fwd,
        carried_bwd,
        decay_cum,
        decay_total,
        before,
        after_sum,
        query_blocks,
    )
    return (pieces, (summary_fwd, summary_bwd, overall))


def finish_terms(pieces, incoming_fwd, incoming_bwd):
    (
        near_terms,
        carried_fwd,
        carried_bwd,
        decay_cum,
        decay_total,
        before,
        after_sum,
        query_blocks,
    ) = pieces
    total_fwd = carried_fwd + jnp.exp(before)[..., None, None] * incoming_fwd[None]
    total_bwd = carried_bwd + jnp.exp(after_sum)[..., None, None] * incoming_bwd[None]
    query_wide = query_blocks.astype(jnp.float32)
    read_fwd = jnp.einsum(
        "kign,kgrnp->kigrp", query_wide, total_fwd, precision=lax.Precision.HIGHEST
    )
    read_bwd = jnp.einsum(
        "kign,kgrnp->kigrp", query_wide, total_bwd, precision=lax.Precision.HIGHEST
    )
    combined = (
        near_terms
        + jnp.exp(decay_cum)[..., None] * read_fwd
        + jnp.exp(decay_total[:, None] - decay_cum)[..., None] * read_bwd
    )
    block_count, block_len, group_count, head_ratio, head_dim = combined.shape
    return combined.reshape(block_count * block_len, group_count, head_ratio, head_dim)


def combine_all(gathered_states, own_index):
    after_all, before_all, logs_all = gathered_states
    device_count = logs_all.shape[0]
    cum_incl = jnp.cumsum(logs_all, axis=0)
    cum_excl = cum_incl - logs_all
    device_order = jnp.arange(device_count)
    picker = (device_order == own_index).astype(jnp.float32)[:, None, None]
    own_incl = jnp.sum(picker * cum_incl, axis=0)
    own_excl = jnp.sum(picker * cum_excl, axis=0)
    lower_mask = (device_order < own_index)[:, None, None]
    higher_mask = (device_order > own_index)[:, None, None]
    weight_fwd = jnp.where(lower_mask, jnp.exp(jnp.minimum(own_excl[None] - cum_incl, 0.0)), 0.0)
    weight_bwd = jnp.where(higher_mask, jnp.exp(jnp.minimum(cum_excl - own_incl[None], 0.0)), 0.0)
    incoming_fwd = jnp.einsum(
        "dgr,dgrnp->grnp", weight_fwd, after_all, precision=lax.Precision.HIGHEST
    )
    incoming_bwd = jnp.einsum(
        "dgr,dgrnp->grnp", weight_bwd, before_all, precision=lax.Precision.HIGHEST
    )
    return (incoming_fwd, incoming_bwd)


def shards(
    tokens,
    norm_gain,
    state_gate,
    state_value,
    state_keys,
    state_query,
    state_step,
    state_rate,
    state_jumps,
    state_gain,
    filter_value,
    filter_keys,
    filter_query,
    window_query,
    window_keys,
    window_values,
    window_sink,
    state_output,
    window_output,
):
    row_count = tokens.shape[0]
    rows_wide = tokens.astype(jnp.float32)
    normed = (
        rows_wide
        * lax.rsqrt(jnp.mean(rows_wide * rows_wide, axis=-1, keepdims=True) + 1e-06)
        * norm_gain
    ).astype(jnp.bfloat16)
    gathered = (
        lax.all_gather(state_gate, "sp", axis=0, tiled=True),
        lax.all_gather(state_value, "sp", axis=0, tiled=True),
        lax.all_gather(state_keys, "sp", axis=0, tiled=True),
        lax.all_gather(state_query, "sp", axis=0, tiled=True),
        lax.all_gather(window_query, "sp", axis=0, tiled=True),
        lax.all_gather(window_keys, "sp", axis=0, tiled=True),
        lax.all_gather(window_values, "sp", axis=0, tiled=True),
        lax.all_gather(state_output, "sp", axis=1, tiled=True),
        lax.all_gather(window_output, "sp", axis=1, tiled=True),
    )
    projected = [
        jnp.dot(normed, matrix, preferred_element_type=jnp.float32) for matrix in gathered[:7]
    ]
    out_state = gathered[7]
    out_window = gathered[8]
    gate_rows, value_pre, keys_pre, query_pre, query_raw, keys_raw, values_rows = [
        result.astype(jnp.bfloat16) for result in projected
    ]
    head_local = state_rate.shape[0]
    group_local = keys_pre.shape[1] // STATE_SIZE
    head_dim = value_pre.shape[1] // head_local
    head_ratio = head_local // group_local
    step_cols = lax.dynamic_slice_in_dim(
        state_step, lax.axis_index("tp") * head_local, head_local, 1
    )
    step_rows = jax.nn.softplus(jnp.dot(normed, step_cols, preferred_element_type=jnp.float32))
    log_decay = -state_rate[None, :] * step_rows + state_jumps
    half_width = filter_value.shape[0] // 2
    stacked = jnp.concatenate([value_pre, keys_pre, query_pre], axis=-1)
    padded = extended(stacked, (("sp", 0),), half_width)
    filters = jnp.concatenate([filter_value, filter_keys, filter_query], axis=-1).astype(
        jnp.float32
    )
    filtered = jnp.zeros(stacked.shape, jnp.float32)
    for offset in range(filters.shape[0]):
        filtered = (
            filtered + padded[offset : offset + row_count].astype(jnp.float32) * filters[offset]
        )
    value_cols = value_pre.shape[1]
    key_cols = keys_pre.shape[1]
    inner_rows = (
        jax.nn.silu(filtered[:, :value_cols]).reshape(row_count, head_local, head_dim)
        * step_rows[..., None]
    )
    scan_values = inner_rows.astype(jnp.bfloat16).reshape(
        row_count, group_local, head_ratio, head_dim
    )
    scan_keys = (
        filtered[:, value_cols : value_cols + key_cols]
        .astype(jnp.bfloat16)
        .reshape(row_count, group_local, STATE_SIZE)
    )
    scan_query = (
        filtered[:, value_cols + key_cols :]
        .astype(jnp.bfloat16)
        .reshape(row_count, group_local, STATE_SIZE)
    )
    pieces, summaries = block_terms(
        scan_query,
        scan_keys,
        scan_values,
        log_decay.reshape(row_count, group_local, head_ratio),
        BLOCK,
    )
    summary_fwd, summary_bwd, overall = summaries
    gathered_states = (
        lax.all_gather(summary_fwd[None].astype(jnp.bfloat16), "sp", axis=0, tiled=True).astype(
            jnp.float32
        ),
        lax.all_gather(summary_bwd[None].astype(jnp.bfloat16), "sp", axis=0, tiled=True).astype(
            jnp.float32
        ),
        lax.all_gather(overall[None].astype(jnp.bfloat16), "sp", axis=0, tiled=True).astype(
            jnp.float32
        ),
    )
    incoming_fwd, incoming_bwd = combine_all(gathered_states, lax.axis_index("sp"))
    scan_out = finish_terms(pieces, incoming_fwd, incoming_bwd).reshape(
        row_count, head_local * head_dim
    )
    gated_rows = scan_out * jax.nn.silu(gate_rows.astype(jnp.float32))
    per_head = gated_rows.reshape(row_count, head_local, head_dim)
    state_mix = (
        (
            per_head
            * lax.rsqrt(jnp.mean(per_head * per_head, axis=-1, keepdims=True) + 1e-06)
            * state_gain.reshape(head_local, head_dim)
        )
        .astype(jnp.bfloat16)
        .reshape(row_count, head_local * head_dim)
    )
    query_heads = window_sink.shape[0]
    kv_heads = keys_raw.shape[1] // HEAD_DIM
    kv_width = kv_heads * HEAD_DIM
    positions = lax.axis_index("sp") * row_count + jnp.arange(row_count, dtype=jnp.int32)
    query_rot = rotate_grid(
        query_raw.reshape(row_count, query_heads, HEAD_DIM), positions, GRID_WIDTH
    )
    keys_rot = rotate_grid(keys_raw.reshape(row_count, kv_heads, HEAD_DIM), positions, GRID_WIDTH)
    pair_rows = jnp.concatenate([keys_rot.reshape(row_count, kv_width), values_rows], axis=-1)
    padded_pair = extended(pair_rows, (("sp", 0),), WINDOW)
    keys_pad = padded_pair[:, :kv_width].reshape(-1, kv_heads, HEAD_DIM)
    values_pad = padded_pair[:, kv_width:].reshape(-1, kv_heads, HEAD_DIM)
    window_mix = window_attend(
        query_rot,
        keys_pad,
        values_pad,
        window_sink,
        lax.axis_index("sp") * row_count - WINDOW,
        lax.axis_size("sp") * row_count,
        WINDOW,
    )
    return lax.psum_scatter(
        (
            jnp.dot(state_mix, out_state, preferred_element_type=jnp.float32)
            + jnp.dot(window_mix, out_window, preferred_element_type=jnp.float32)
        ).astype(jnp.bfloat16),
        "tp",
        scatter_dimension=0,
        tiled=True,
    )


def solution(mesh):
    placed = (
        P(("fs", "sp"), None),
        P(),
        P("sp", "tp"),
        P("sp", "tp"),
        P("sp", "tp"),
        P("sp", "tp"),
        P(),
        P("tp"),
        P(("fs", "sp"), "tp"),
        P("tp"),
        P(None, "tp"),
        P(None, "tp"),
        P(None, "tp"),
        P("sp", "tp"),
        P("sp", "tp"),
        P("sp", "tp"),
        P("tp"),
        P("tp", "sp"),
        P("tp", "sp"),
    )
    return jax.shard_map(
        shards, mesh=mesh, in_specs=placed, out_specs=P(("fs", "sp", "tp"), None), check_vma=False
    )
```

profile of v0, /device:TPU:0, one launch (start us, length us, event | category | flops | bytes accessed | tf_op | source)
XLA Modules:
  0.0 539.9 jit_solution(15252986102147311242)
XLA Ops:
  20.1 13.3 %all-gather.3 = bf16[4,4,2]{1,2,0:T(2,128)(2,1)S(1)} all-gather(bf16[1,4,2]{1,2,0:T(2,128)(2,1)S(1)} %convert_bitcast_fusion), channel_id=2, replica_groups=mesh['sp'=4,'fs'=4,'tp'=2] {'sp'}, dimensions={0}, use_global_device_ids=true | all-gather | bytes 80 | tf_op jit(solution)/shard_map/all_gather | solution.py:308
  40.1 17.2 %all-gather.24.cloned.1.call-done = bf16[2048,512]{1,0:T(8,128)(2,1)} async-done(((bf16[512,512]{1,0:T(8,128)(2,1)}), bf16[2048,512]{1,0:T(8,128)(2,1)}) %all-gather.24.cloned.1.call-update) | async-done | bytes 2097168 | tf_op jit(solution)/shard_map/all_gather | solution.py:241
  60.4 43.0 %all-gather.18.cloned.1.call-done = bf16[2048,512]{1,0:T(8,128)(2,1)} async-done(((bf16[512,512]{1,0:T(8,128)(2,1)}), bf16[2048,512]{1,0:T(8,128)(2,1)}) %all-gather.18.cloned.1.call-update) | async-done | bytes 2097168 | tf_op jit(solution)/shard_map/all_gather | solution.py:239
  103.4 3.6 convolution_convert_fusion.4
  107.0 42.5 %all-gather.16.cloned.1.call-done = bf16[2048,512]{1,0:T(8,128)(2,1)} async-done(((bf16[512,512]{1,0:T(8,128)(2,1)}), bf16[2048,512]{1,0:T(8,128)(2,1)}) %all-gather.16.cloned.1.call-update) | async-done | bytes 2097168 | tf_op jit(solution)/shard_map/all_gather | solution.py:238
  149.5 3.6 convolution_convert_fusion.5
  153.1 42.3 %all-gather.14.cloned.1.call-done = bf16[2048,512]{1,0:T(8,128)(2,1)} async-done(((bf16[512,512]{1,0:T(8,128)(2,1)}), bf16[2048,512]{1,0:T(8,128)(2,1)}) %all-gather.14.cloned.1.call-update) | async-done | bytes 2097168 | tf_op jit(solution)/shard_map/all_gather | solution.py:237
  195.4 3.6 convolution_convert_fusion.6
  205.2 44.7 %all-gather.26.cloned.1.call-done = bf16[2048,512]{1,0:T(8,128)(2,1)} async-done(((bf16[512,512]{1,0:T(8,128)(2,1)}), bf16[2048,512]{1,0:T(8,128)(2,1)}) %all-gather.26.cloned.1.call-update) | async-done | bytes 2097168 | tf_op jit(solution)/shard_map/all_gather | solution.py:242
  249.9 3.6 convolution_convert_fusion.1
  261.8 5.9 %maximum_maximum_fusion = (bf16[514,1536]{0,1:T(8,128)(2,1)S(1)}, bf16[514,1536]{0,1:T(8,128)(2,1)S(1)}) fusion(bf16[512,512]{0,1:T(8,128)(2,1)S(1)} %convolution_convert_fusion.4, bf16[512,512]{0,1:T(8,128)(2,1)S(1)} %convolution_convert_fusion.5, bf16[512,512]{0,1:T(8,128)(2,1)S(1)} %convolution_convert_fusion.6, bf16[2,1536]{0,1:T(8,128)(2,1)} %collective-permute-done, ...), kind=kLoop, calls=%fused_computation.19 | loop fusion | flops 12632064 | bytes 4743168 | tf_op jit(solution)/shard_map/concatenate | solution.py:19
  267.7 5.8 %fusion.122 = (bf16[512,1536]{0,1:T(8,128)(2,1)}, f32[512,1536]{0,1:T(8,128)S(1)}) fusion(f32[1536]{0:T(1024)S(1)} %get-tuple-element.9, bf16[514,1536]{0,1:T(8,128)(2,1)S(1)} %get-tuple-element.19, f32[1536]{0:T(1024)S(1)} %get-tuple-element.6, f32[1536]{0:T(1024)S(1)} %get-tuple-element.7, bf16[512,512]{0,1:T(8,128)(2,1)S(1)} %convolution_convert_fusion.4, ...), kind=kLoop, calls=%fused_computation.221 | loop fusion | flops 15728640 | bytes 12613632 | tf_op jit(solution)/shard_map/convert.2
  284.0 23.4 %all-gather.1 = bf16[16,2,128,64]{2,3,1,0:T(8,128)(2,1)S(1)} all-gather(bf16[4,2,128,64]{2,3,1,0:T(8,128)(2,1)S(1)} %get-tuple-element.59), channel_id=3, replica_groups=mesh['sp'=4,'fs'=4,'tp'=2] {'sp'}, dimensions={0}, use_global_device_ids=true | all-gather | bytes 655360 | tf_op jit(solution)/shard_map/all_gather | solution.py:302
  308.5 16.1 %all-gather.2 = bf16[16,2,128,64]{2,3,1,0:T(8,128)(2,1)S(1)} all-gather(bf16[4,2,128,64]{2,3,1,0:T(8,128)(2,1)S(1)} %get-tuple-element.62), channel_id=4, replica_groups=mesh['sp'=4,'fs'=4,'tp'=2] {'sp'}, dimensions={0}, use_global_device_ids=true | all-gather | bytes 655360 | tf_op jit(solution)/shard_map/all_gather | solution.py:305
  334.8 3.9 bitcast_reduce_fusion
  346.6 45.2 %all-gather.28.cloned.1.call-done = bf16[2048,1024]{1,0:T(8,128)(2,1)} async-done(((bf16[512,1024]{1,0:T(8,128)(2,1)}), bf16[2048,1024]{1,0:T(8,128)(2,1)}) %all-gather.28.cloned.1.call-update) | async-done | bytes 4194320 | tf_op jit(solution)/shard_map/all_gather | solution.py:240
  391.8 5.4 %convolution_convert_fusion = bf16[512,1024]{1,0:T(8,128)(2,1)S(1)} fusion(bf16[2048,1024]{1,0:T(8,128)(2,1)} %all-gather.28.cloned.1.call-done, bf16[512,2048]{1,0:T(8,128)(2,1)} %param.19, f32[2048]{0:T(1024)S(1)} %copy-done.23, f32[512]{0:T(512)S(1)} %copy-done.17), kind=kOutput, calls=%fused_computation.34 | convolution fusion | flops 2152202240 | bytes 7350272 | tf_op jit(solution)/shard_map/dot_general | solution.py:247
  397.2 3.1 reshape.412
  408.4 5.3 fusion
  419.9 52.7 %all-gather.30.cloned.1.call-done = bf16[1024,2048]{1,0:T(8,128)(2,1)} async-done(((bf16[1024,512]{1,0:T(8,128)(2,1)}), bf16[1024,2048]{1,0:T(8,128)(2,1)}) %all-gather.30.cloned.1.call-update) | async-done | bytes 4194320 | tf_op jit(solution)/shard_map/all_gather | solution.py:244
  472.6 6.5 %fusion.128 = f32[512,2048]{1,0:T(8,128)} fusion(bf16[512,1024]{1,0:T(8,128)(2,1)S(1)} %convert_element_type.224, bf16[1024,2048]{1,0:T(8,128)(2,1)} %all-gather.30.cloned.1.call-done), kind=kOutput, calls=%fused_computation.227 | convolution fusion | flops 2147483648 | bytes 9437184 | tf_op jit(solution)/shard_map/dot_general | solution.py:351
  479.2 39.2 %all-gather.22.cloned.1.call-done = bf16[512,2048]{1,0:T(8,128)(2,1)} async-done(((bf16[512,512]{1,0:T(8,128)(2,1)}), bf16[512,2048]{1,0:T(8,128)(2,1)}) %all-gather.22.cloned.1.call-update) | async-done | bytes 2097168 | tf_op jit(solution)/shard_map/all_gather | solution.py:243
  518.4 5.5 %add_convert_fusion = bf16[512,2048]{1,0:T(8,128)(2,1)} fusion(f32[512,2048]{1,0:T(8,128)} %fusion.128, bf16[512,512]{0,1:T(8,128)(2,1)S(1)} %fusion.41, bf16[512,2048]{1,0:T(8,128)(2,1)} %all-gather.22.cloned.1.call-done), kind=kOutput, calls=%fused_computation.10 | convolution fusion | flops 1075838976 | bytes 8912896 | tf_op jit(solution)/shard_map/dot_general | solution.py:350
  523.9 8.7 %reduce-scatter.2.cloned.1.call-done = bf16[256,2048]{1,0:T(8,128)(2,1)} async-done(((bf16[512,2048]{1,0:T(8,128)(2,1)}), bf16[256,2048]{1,0:T(8,128)(2,1)}) %reduce-scatter.2.cloned.1.call-update) | async-done | bytes 1048592 | tf_op jit(solution)/shard_map/reduce_scatter | solution.py:348
  (184 shorter events, 81.0 us)
Async XLA Ops:
  6.5 6.9 %copy-start = (bf16[2048,16]{0,1:T(8,128)(2,1)S(1)}, bf16[2048,16]{0,1:T(8,128)(2,1)}, u32[]{:S(2)}) copy-start(bf16[2048,16]{0,1:T(8,128)(2,1)} %param.25) | copy-start | bytes 196612
  6.5 50.8 %all-gather.24.cloned.1.call-start = ((), (), s32[]{:S(2)}) async-start(), calls=%async_computation.6 | async-start | bytes 2621440 | tf_op jit(solution)/shard_map/all_gather | solution.py:241
  7.3 96.2 %all-gather.18.cloned.1.call-start = ((), (), s32[]{:S(2)}) async-start(), calls=%async_computation.3 | async-start | bytes 2621440 | tf_op jit(solution)/shard_map/all_gather | solution.py:239
  8.0 141.5 %all-gather.16.cloned.1.call-start = ((), (), s32[]{:S(2)}) async-start(), calls=%async_computation.2 | async-start | bytes 2621440 | tf_op jit(solution)/shard_map/all_gather | solution.py:238
  8.8 186.6 %all-gather.14.cloned.1.call-start = ((), (), s32[]{:S(2)}) async-start(), calls=%async_computation.1 | async-start | bytes 2621440 | tf_op jit(solution)/shard_map/all_gather | solution.py:237
  9.4 240.6 %all-gather.26.cloned.1.call-start = ((), (), s32[]{:S(2)}) async-start(), calls=%async_computation.7 | async-start | bytes 2621440 | tf_op jit(solution)/shard_map/all_gather | solution.py:242
  9.9 324.9 %all-gather.20.cloned.1.call-start = ((), (), s32[]{:S(2)}) async-start(), calls=%async_computation.4 | async-start | bytes 2621440 | tf_op jit(solution)/shard_map/all_gather | solution.py:236
  10.5 381.2 %all-gather.28.cloned.1.call-start = ((), (), s32[]{:S(2)}) async-start(), calls=%async_computation.8 | async-start | bytes 5242880 | tf_op jit(solution)/shard_map/all_gather | solution.py:240
  11.3 461.3 %all-gather.30.cloned.1.call-start = ((), (), s32[]{:S(2)}) async-start(), calls=%async_computation.9 | async-start | bytes 5242880 | tf_op jit(solution)/shard_map/all_gather | solution.py:244
  12.0 506.4 %all-gather.22.cloned.1.call-start = ((), (), s32[]{:S(2)}) async-start(), calls=%async_computation.5 | async-start | bytes 2621440 | tf_op jit(solution)/shard_map/all_gather | solution.py:243
  12.8 519.8 %reduce-scatter.2.cloned.1.call-start = ((), (), s32[]{:S(2)}) async-start(), calls=%async_computation.10 | async-start | bytes 3145728 | tf_op jit(solution)/shard_map/reduce_scatter | solution.py:348
  20.1 37.3 %copy-start.4 = (bf16[512,2048]{1,0:T(8,128)(2,1)S(1)}, bf16[512,2048]{1,0:T(8,128)(2,1)}, u32[]{:S(2)}) copy-start(bf16[512,2048]{1,0:T(8,128)(2,1)} %param.19) | copy-start | bytes 6291460
  40.1 63.3 %copy-start.17 = (f32[512]{0:T(512)S(1)}, f32[512]{0:T(512)}, u32[]{:S(2)}) copy-start(f32[512]{0:T(512)} %copy-done.16) | copy-start | bytes 6148
  40.1 63.3 %copy-start.23 = (f32[2048]{0:T(1024)S(1)}, f32[2048]{0:T(1024)}, u32[]{:S(2)}) copy-start(f32[2048]{0:T(1024)} %param.20) | copy-start | bytes 24580
  200.2 61.6 %collective-permute-start = (bf16[2,1536]{0,1:T(8,128)(2,1)}, bf16[2,1536]{0,1:T(8,128)(2,1)}, u32[]{:S(2)}, u32[]{:S(2)}) collective-permute-start(bf16[2,1536]{0,1:T(8,128)(2,1)} %get-tuple-element.20), channel_id=1, source_target_pairs={{0,8},{8,16},{16,24},{1,9},{9,17},{17,25},{2,10},{10,18},{18,26},{... | collective-permute-start | bytes 18440 | tf_op jit(solution)/shard_map/ppermute | solution.py:21
  203.0 58.8 %collective-permute-start.1 = (bf16[2,1536]{0,1:T(8,128)(2,1)}, bf16[2,1536]{0,1:T(8,128)(2,1)}, u32[]{:S(2)}, u32[]{:S(2)}) collective-permute-start(bf16[2,1536]{0,1:T(8,128)(2,1)} %get-tuple-element.21), channel_id=1, source_target_pairs={{8,0},{16,8},{24,16},{9,1},{17,9},{25,17},{10,2},{18,10},{26,18},{... | collective-permute-start | bytes 18440 | tf_op jit(solution)/shard_map/ppermute | solution.py:23
  255.4 83.5 %collective-permute-start.2 = (bf16[128,1024]{0,1:T(8,128)(2,1)}, bf16[128,1024]{0,1:T(8,128)(2,1)S(1)}, u32[]{:S(2)}, u32[]{:S(2)}) collective-permute-start(bf16[128,1024]{0,1:T(8,128)(2,1)} %get-tuple-element.37), channel_id=1, source_target_pairs={{0,8},{8,16},{16,24},{1,9},{9,17},{17,25},{2,10},{10,18},{18,26},{... | collective-permute-start | bytes 786440 | tf_op jit(solution)/shard_map/ppermute | solution.py:21
  257.4 81.5 %collective-permute-start.3 = (bf16[128,1024]{0,1:T(8,128)(2,1)}, bf16[128,1024]{0,1:T(8,128)(2,1)}, u32[]{:S(2)}, u32[]{:S(2)}) collective-permute-start(bf16[128,1024]{0,1:T(8,128)(2,1)} %get-tuple-element.38), channel_id=1, source_target_pairs={{8,0},{16,8},{24,16},{9,1},{17,9},{25,17},{10,2},{18,10},{26,18},{... | collective-permute-start | bytes 786440 | tf_op jit(solution)/shard_map/ppermute | solution.py:23
  282.8 41.7 %copy-start.6 = (f32[4,4,128,128]{3,2,1,0:T(8,128)S(1)}, f32[4,4,128,128]{3,2,1,0:T(8,128)}, u32[]{:S(2)}) copy-start(f32[4,4,128,128]{3,2,1,0:T(8,128)} %fusion.56) | copy-start | bytes 3145732
  282.9 41.7 %copy-start.12 = (f32[4,4,2,128]{3,2,1,0:T(2,128)S(1)}, f32[4,4,2,128]{3,2,1,0:T(2,128)}, u32[]{:S(2)}) copy-start(f32[4,4,2,128]{3,2,1,0:T(2,128)} %copy.184) | copy-start | bytes 49156
  308.5 17.8 %copy-start.14 = (f32[4,4,2]{0,2,1:T(2,128)S(1)}, f32[4,4,2]{0,2,1:T(2,128)}, u32[]{:S(2)}) copy-start(f32[4,4,2]{0,2,1:T(2,128)} %copy.195) | copy-start | bytes 388
  308.5 17.8 %copy-start.20 = (pred[4,4]{1,0:T(4,128)(4,1)S(1)}, pred[4,4]{1,0:T(4,128)(4,1)}, u32[]{:S(2)}) copy-start(pred[4,4]{1,0:T(4,128)(4,1)} %iota_compare_fusion.1) | copy-start | bytes 52
  401.7 6.7 %copy-start.5 = (f32[4,128,4,2,128]{4,3,2,1,0:T(2,128)S(1)}, f32[4,128,4,2,128]{4,3,2,1,0:T(2,128)}, u32[]{:S(2)}) copy-start(f32[4,128,4,2,128]{4,3,2,1,0:T(2,128)} %reshape.412) | copy-start | bytes 6291460
  518.4 14.2 %copy-start.1 = (bf16[2048,16]{0,1:T(8,128)(2,1)S(1)}, bf16[2048,16]{0,1:T(8,128)(2,1)}, u32[]{:S(2)}) copy-start(bf16[2048,16]{0,1:T(8,128)(2,1)} %param.25) | copy-start | bytes 196612
  (15 other events, 52.8 us)
Sparse Core Ops, SparseCore 0:
  8.9 48.4 all-gather.23
  58.9 44.4 all-gather.17
  105.0 44.4 all-gather.15
  150.9 44.4 all-gather.13
  196.8 53.0 all-gather.25
  251.3 58.3 all-gather.19
  311.3 80.3 all-gather.27
  393.3 79.2 all-gather.29
  474.2 44.1 all-gather.21
  524.0 8.5 reduce-scatter.1
where the time goes:
time: 549 us; the launch traced here: 540 us
  waiting for transfers between devices  341 us (62%)
  matrix products  60.4 us (11%)
  blocking collectives  52.7 us (10%)
  local copies, waits for them, and re-layouts  33.6 us (6%)
  other arithmetic  28.8 us (5%)
  between operations  14.7 us (3%)
  starting transfers between devices  8.28 us (2%)
    all_gather x1, waiting for transfers between devices, shards(): lax.all_gather(window_output, 'sp', axis=1, tiled=True)  52.7 us
    all_gather x1, waiting for transfers between devices, shards(): lax.all_gather(window_query, 'sp', axis=0, tiled=True)  45.2 us
    all_gather x1, waiting for transfers between devices, shards(): lax.all_gather(window_values, 'sp', axis=0, tiled=True)  44.7 us
    all_gather x1, waiting for transfers between devices, shards(): lax.all_gather(state_query, 'sp', axis=0, tiled=True)  43 us
    all_gather x1, waiting for transfers between devices, shards(): lax.all_gather(state_keys, 'sp', axis=0, tiled=True)  42.5 us
    all_gather x1, waiting for transfers between devices, shards(): lax.all_gather(state_value, 'sp', axis=0, tiled=True)  42.3 us
    all_gather x1, waiting for transfers between devices, shards(): lax.all_gather(state_output, 'sp', axis=1, tiled=True)  39.2 us
    dot_general x7, matrix products, shards(): jnp.dot(normed, matrix, preferred_element_type=jnp.float32)  26.7 us
  transfers between devices with their start and end apart: 14, of which 9 were waited for; matrix products, arithmetic and copies ran while one was open for 22% of the time, Pallas kernels for 0%

commit v1 on v0

--- a/solution.py
+++ b/solution.py
@@ -8,6 +8,16 @@
 WINDOW = 128
 BLOCK = 128
 GRID_WIDTH = 64
+
+
+def gather_around(x, axis, dim):
+    ways, here, lap = (lax.axis_size(axis), lax.axis_index(axis), x.shape[dim])
+    shape = [n * ways if d == dim else n for d, n in enumerate(x.shape)]
+    full = lax.dynamic_update_slice_in_dim(jnp.zeros(shape, x.dtype), x, here * lap, axis=dim)
+    for far in range(1, ways):
+        x = lax.ppermute(x, axis, [(d, (d + 1) % ways) for d in range(ways)])
+        full = lax.dynamic_update_slice_in_dim(full, x, (here - far) % ways * lap, axis=dim)
+    return full
 
 
 def extended(cells, sides, width):
@@ -236,7 +246,7 @@
         lax.all_gather(state_gate, "sp", axis=0, tiled=True),
         lax.all_gather(state_value, "sp", axis=0, tiled=True),
         lax.all_gather(state_keys, "sp", axis=0, tiled=True),
-        lax.all_gather(state_query, "sp", axis=0, tiled=True),
+        gather_around(state_query, "sp", 0),
         lax.all_gather(window_query, "sp", axis=0, tiled=True),
         lax.all_gather(window_keys, "sp", axis=0, tiled=True),
         lax.all_gather(window_values, "sp", axis=0, tiled=True),

time: 549 us -> 516 us (0.940)
  waiting for transfers between devices: 341 us -> 287 us
  blocking collectives: 52.7 us -> 67.6 us
  local copies, waits for them, and re-layouts: 33.6 us -> 39.6 us
    all_gather x1 -> x0, waiting for transfers between devices: 43 us -> none  [shards(): lax.all_gather(state_query, 'sp', axis=0, tiled=True)]
    ppermute x0 -> x3, waiting for transfers between devices: none -> 26.2 us  [gather_around(): x = lax.ppermute(x, axis, [(d, (d + 1) % ways) for d in range(ways)])]
    all_gather x1, waiting for transfers between devices: 42.5 us -> 22.6 us  [shards(): lax.all_gather(state_keys, 'sp', axis=0, tiled=True)]
    all_gather x1, waiting for transfers between devices: 17.2 us -> 0.02 us  [shards(): lax.all_gather(window_keys, 'sp', axis=0, tiled=True)]
    all_gather x1, blocking collectives: 13.3 us -> 27.3 us  [shards(): lax.all_gather(overall[None].astype(jnp.bfloat16), 'sp', axis=0, tiled=True)]
    dynamic_update_slice x0 -> x4, local copies, waits for them, and re-layouts: none -> 5.66 us  [the longest x3 5.62 us: gather_around(): lax.dynamic_update_slice_in_dim(full, x, (here - far) % ways * lap, axis=...]
  transfers between devices with their start and end apart: 14 -> 16, of which waited for: 9 -> 9; matrix products, arithmetic and copies ran while one was open for 22% -> 24% of each run, Pallas kernels for 0% -> 0%
where the time goes in v1:
time: 516 us; the launch traced here: 512 us
  waiting for transfers between devices  287 us (56%)
  blocking collectives  67.6 us (13%)
  matrix products  60.7 us (12%)
  local copies, waits for them, and re-layouts  39.6 us (8%)
  other arithmetic  30.7 us (6%)
  between operations  14.3 us (3%)
  starting transfers between devices  11.8 us (2%)
    all_gather x1, waiting for transfers between devices, shards(): lax.all_gather(window_output, 'sp', axis=1, tiled=True)  54.4 us
    all_gather x1, waiting for transfers between devices, shards(): lax.all_gather(window_values, 'sp', axis=0, tiled=True)  45.2 us
    all_gather x1, waiting for transfers between devices, shards(): lax.all_gather(window_query, 'sp', axis=0, tiled=True)  43.2 us
    all_gather x1, waiting for transfers between devices, shards(): lax.all_gather(state_value, 'sp', axis=0, tiled=True)  42.7 us
    all_gather x1, waiting for transfers between devices, shards(): lax.all_gather(state_output, 'sp', axis=1, tiled=True)  39.2 us
    all_gather x1, blocking collectives, shards(): lax.all_gather(overall[None].astype(jnp.bfloat16), 'sp', axis=0, tiled=True)  27.3 us
    dot_general x7, matrix products, shards(): jnp.dot(normed, matrix, preferred_element_type=jnp.float32)  27 us
    ppermute x3, waiting for transfers between devices, gather_around(): x = lax.ppermute(x, axis, [(d, (d + 1) % ways) for d in range(ways)])  26.2 us
  transfers between devices with their start and end apart: 16, of which 9 were waited for; matrix products, arithmetic and copies ran while one was open for 24% of the time, Pallas kernels for 0%

profile of v1, /device:TPU:0, one launch (start us, length us, event | category | flops | bytes accessed | tf_op | source)
XLA Modules:
  0.0 511.5 jit_solution(17827374446706327498)
XLA Ops:
  18.0 27.3 %all-gather.3 = bf16[4,4,2]{1,2,0:T(2,128)(2,1)S(1)} all-gather(bf16[1,4,2]{1,2,0:T(2,128)(2,1)S(1)} %convert_bitcast_fusion), channel_id=2, replica_groups=mesh['sp'=4,'fs'=4,'tp'=2] {'sp'}, dimensions={0}, use_global_device_ids=true | all-gather | bytes 80 | tf_op jit(solution)/shard_map/all_gather | solution.py:318
  51.2 22.6 %collective-permute-done.1 = bf16[512,512]{1,0:T(8,128)(2,1)} collective-permute-done((bf16[512,512]{1,0:T(8,128)(2,1)}, bf16[512,512]{1,0:T(8,128)(2,1)}, u32[]{:S(2)}, u32[]{:S(2)}) %collective-permute-start.1) | collective-permute-done | bytes 524320 | tf_op jit(solution)/shard_map/ppermute | solution.py:18
  85.4 3.6 collective-permute-done.2
  90.9 3.6 convolution_convert_fusion.4
  94.6 3.6 convolution_convert_fusion.2
  98.3 22.6 %all-gather.15.cloned.1.call-done = bf16[2048,512]{1,0:T(8,128)(2,1)} async-done(((bf16[512,512]{1,0:T(8,128)(2,1)}), bf16[2048,512]{1,0:T(8,128)(2,1)}) %all-gather.15.cloned.1.call-update) | async-done | bytes 2097168 | tf_op jit(solution)/shard_map/all_gather | solution.py:248
  120.9 3.6 convolution_convert_fusion.5
  124.5 42.7 %all-gather.13.cloned.1.call-done = bf16[2048,512]{1,0:T(8,128)(2,1)} async-done(((bf16[512,512]{1,0:T(8,128)(2,1)}), bf16[2048,512]{1,0:T(8,128)(2,1)}) %all-gather.13.cloned.1.call-update) | async-done | bytes 2097168 | tf_op jit(solution)/shard_map/all_gather | solution.py:247
  167.3 3.6 convolution_convert_fusion.6
  176.6 45.2 %all-gather.23.cloned.1.call-done = bf16[2048,512]{1,0:T(8,128)(2,1)} async-done(((bf16[512,512]{1,0:T(8,128)(2,1)}), bf16[2048,512]{1,0:T(8,128)(2,1)}) %all-gather.23.cloned.1.call-update) | async-done | bytes 2097168 | tf_op jit(solution)/shard_map/all_gather | solution.py:252
  221.8 3.6 convolution_convert_fusion.1
  234.3 5.9 %maximum_maximum_fusion = (bf16[514,1536]{0,1:T(8,128)(2,1)S(1)}, bf16[514,1536]{0,1:T(8,128)(2,1)S(1)}) fusion(bf16[512,512]{0,1:T(8,128)(2,1)S(1)} %convolution_convert_fusion.4, bf16[512,512]{0,1:T(8,128)(2,1)S(1)} %convolution_convert_fusion.5, bf16[512,512]{0,1:T(8,128)(2,1)S(1)} %convolution_convert_fusion.6, ...), kind=kLoop, calls=%fused_computation.19 | loop fusion | flops 12632064 | bytes 4743168 | tf_op jit(solution)/shard_map/concatenate | solution.py:29
  240.2 5.8 %fusion.122 = (bf16[512,1536]{0,1:T(8,128)(2,1)}, f32[512,1536]{0,1:T(8,128)S(1)}) fusion(f32[1536]{0:T(1024)S(1)} %copy-done.16, bf16[514,1536]{0,1:T(8,128)(2,1)S(1)} %get-tuple-element.19, f32[1536]{0:T(1024)S(1)} %get-tuple-element.6, f32[1536]{0:T(1024)S(1)} %copy-done.14, bf16[512,512]{0,1:T(8,128)(2,1)S(1)} %convolution_convert_fusion.4, ...), kind=kLoop, calls=%fused_computation.225 | loop fusion | flops 15728640 | bytes 12613632 | tf_op jit(solution)/shard_map/convert.2
  256.6 23.5 %all-gather.1 = bf16[16,2,128,64]{2,3,1,0:T(8,128)(2,1)S(1)} all-gather(bf16[4,2,128,64]{2,3,1,0:T(8,128)(2,1)S(1)} %get-tuple-element.59), channel_id=3, replica_groups=mesh['sp'=4,'fs'=4,'tp'=2] {'sp'}, dimensions={0}, use_global_device_ids=true | all-gather | bytes 655360 | tf_op jit(solution)/shard_map/all_gather | solution.py:312
  281.2 16.8 %all-gather.2 = bf16[16,2,128,64]{2,3,1,0:T(8,128)(2,1)S(1)} all-gather(bf16[4,2,128,64]{2,3,1,0:T(8,128)(2,1)S(1)} %get-tuple-element.62), channel_id=4, replica_groups=mesh['sp'=4,'fs'=4,'tp'=2] {'sp'}, dimensions={0}, use_global_device_ids=true | all-gather | bytes 655360 | tf_op jit(solution)/shard_map/all_gather | solution.py:315
  309.3 3.5 bitcast_reduce_fusion
  320.6 43.2 %all-gather.25.cloned.1.call-done = bf16[2048,1024]{1,0:T(8,128)(2,1)} async-done(((bf16[512,1024]{1,0:T(8,128)(2,1)}), bf16[2048,1024]{1,0:T(8,128)(2,1)}) %all-gather.25.cloned.1.call-update) | async-done | bytes 4194320 | tf_op jit(solution)/shard_map/all_gather | solution.py:250
  363.9 5.4 %convolution_convert_fusion = bf16[512,1024]{1,0:T(8,128)(2,1)S(1)} fusion(bf16[2048,1024]{1,0:T(8,128)(2,1)} %all-gather.25.cloned.1.call-done, bf16[512,2048]{1,0:T(8,128)(2,1)} %param.19, f32[2048]{0:T(1024)S(1)} %copy-done.32, f32[512]{0:T(512)S(1)} %copy-done.24), kind=kOutput, calls=%fused_computation.34 | convolution fusion | flops 2152202240 | bytes 7350272 | tf_op jit(solution)/shard_map/dot_general | solution.py:257
  378.8 5.4 %fusion = (f32[4,4,2,128]{3,2,1,0:T(2,128)S(1)}, f32[4,4,384,128,2]{3,2,4,1,0:T(8,128)S(1)}) fusion(pred[4,128,384]{1,2,0:T(8,128)(4,1)S(1)} %copy-done.9, f32[4,128,4,2,128]{4,3,2,1,0:T(2,128)S(1)} %copy-done.5, bf16[4,128,4,2,32]{4,1,3,2,0:T(8,128)(2,1)} %copy.223, bf16[4,128,4,2,32]{4,1,3,2,0:T(8,128)(2,1)} %copy.222, ...), kind=kOutput, calls=%fused_computation.3 | convolution fusion | flops 418377728 | bytes 11747328 | tf_op jit(solution)/shard_map/kihgd,kjhd->khgij/dot_general | solution.py:76
  390.4 54.4 %all-gather.27.cloned.1.call-done = bf16[1024,2048]{1,0:T(8,128)(2,1)} async-done(((bf16[1024,512]{1,0:T(8,128)(2,1)}), bf16[1024,2048]{1,0:T(8,128)(2,1)}) %all-gather.27.cloned.1.call-update) | async-done | bytes 4194320 | tf_op jit(solution)/shard_map/all_gather | solution.py:254
  444.7 6.5 %fusion.128 = f32[512,2048]{1,0:T(8,128)} fusion(bf16[512,1024]{1,0:T(8,128)(2,1)S(1)} %convert_element_type.224, bf16[1024,2048]{1,0:T(8,128)(2,1)} %all-gather.27.cloned.1.call-done), kind=kOutput, calls=%fused_computation.231 | convolution fusion | flops 2147483648 | bytes 9437184 | tf_op jit(solution)/shard_map/dot_general | solution.py:361
  451.3 39.2 %all-gather.19.cloned.1.call-done = bf16[512,2048]{1,0:T(8,128)(2,1)} async-done(((bf16[512,512]{1,0:T(8,128)(2,1)}), bf16[512,2048]{1,0:T(8,128)(2,1)}) %all-gather.19.cloned.1.call-update) | async-done | bytes 2097168 | tf_op jit(solution)/shard_map/all_gather | solution.py:253
  490.5 5.5 %add_convert_fusion = bf16[512,2048]{1,0:T(8,128)(2,1)} fusion(f32[512,2048]{1,0:T(8,128)} %fusion.128, bf16[512,512]{0,1:T(8,128)(2,1)S(1)} %fusion.41, bf16[512,2048]{1,0:T(8,128)(2,1)} %all-gather.19.cloned.1.call-done), kind=kOutput, calls=%fused_computation.10 | convolution fusion | flops 1075838976 | bytes 8912896 | tf_op jit(solution)/shard_map/dot_general | solution.py:360
  496.0 8.7 %reduce-scatter.2.cloned.1.call-done = bf16[256,2048]{1,0:T(8,128)(2,1)} async-done(((bf16[512,2048]{1,0:T(8,128)(2,1)}), bf16[256,2048]{1,0:T(8,128)(2,1)}) %reduce-scatter.2.cloned.1.call-update) | async-done | bytes 1048592 | tf_op jit(solution)/shard_map/reduce_scatter | solution.py:358
  (210 shorter events, 91.1 us)
Async XLA Ops:
  6.5 88.1 %all-gather.21.cloned.1.call-start = ((), (), s32[]{:S(2)}) async-start(), calls=%async_computation.5 | async-start | bytes 2621440 | tf_op jit(solution)/shard_map/all_gather | solution.py:251
  7.3 113.7 %all-gather.15.cloned.1.call-start = ((), (), s32[]{:S(2)}) async-start(), calls=%async_computation.2 | async-start | bytes 2621440 | tf_op jit(solution)/shard_map/all_gather | solution.py:248
  8.0 159.3 %all-gather.13.cloned.1.call-start = ((), (), s32[]{:S(2)}) async-start(), calls=%async_computation.1 | async-start | bytes 2621440 | tf_op jit(solution)/shard_map/all_gather | solution.py:247
  8.8 213.0 %all-gather.23.cloned.1.call-start = ((), (), s32[]{:S(2)}) async-start(), calls=%async_computation.6 | async-start | bytes 2621440 | tf_op jit(solution)/shard_map/all_gather | solution.py:252
  9.3 299.9 %all-gather.17.cloned.1.call-start = ((), (), s32[]{:S(2)}) async-start(), calls=%async_computation.3 | async-start | bytes 2621440 | tf_op jit(solution)/shard_map/all_gather | solution.py:246
  9.9 353.9 %all-gather.25.cloned.1.call-start = ((), (), s32[]{:S(2)}) async-start(), calls=%async_computation.7 | async-start | bytes 5242880 | tf_op jit(solution)/shard_map/all_gather | solution.py:250
  10.5 434.2 %all-gather.27.cloned.1.call-start = ((), (), s32[]{:S(2)}) async-start(), calls=%async_computation.8 | async-start | bytes 5242880 | tf_op jit(solution)/shard_map/all_gather | solution.py:254
  11.3 479.2 %all-gather.19.cloned.1.call-start = ((), (), s32[]{:S(2)}) async-start(), calls=%async_computation.4 | async-start | bytes 2621440 | tf_op jit(solution)/shard_map/all_gather | solution.py:253
  11.3 38.2 %collective-permute-start = (bf16[512,512]{1,0:T(8,128)(2,1)S(1)}, bf16[512,512]{1,0:T(8,128)(2,1)}, u32[]{:S(2)}, u32[]{:S(2)}) collective-permute-start(bf16[512,512]{1,0:T(8,128)(2,1)S(1)} %copy-done.13), channel_id=1, source_target_pairs={{0,8},{8,16},{16,24},{24,0},{1,9},{9,17},{17,25},{25,1},{2,10},{10... | collective-permute-start | bytes 1572872 | tf_op jit(solution)/shard_map/ppermute | solution.py:18
  14.5 490.2 %reduce-scatter.2.cloned.1.call-start = ((), (), s32[]{:S(2)}) async-start(), calls=%async_computation.9 | async-start | bytes 3145728 | tf_op jit(solution)/shard_map/reduce_scatter | solution.py:358
  49.2 25.7 %copy-start.25 = (f32[8]{0:T(128)S(1)}, f32[8]{0:T(128)}, u32[]{:S(2)}) copy-start(f32[8]{0:T(128)} %param.35) | copy-start | bytes 100
  49.6 24.2 %collective-permute-start.1 = (bf16[512,512]{1,0:T(8,128)(2,1)}, bf16[512,512]{1,0:T(8,128)(2,1)}, u32[]{:S(2)}, u32[]{:S(2)}) collective-permute-start(bf16[512,512]{1,0:T(8,128)(2,1)} %collective-permute-done), channel_id=1, source_target_pairs={{0,8},{8,16},{16,24},{24,0},{1,9},{9,17},{17,25},{25,1},{2,10},{10... | collective-permute-start | bytes 1572872 | tf_op jit(solution)/shard_map/ppermute | solution.py:18
  73.8 15.3 %collective-permute-start.2 = (bf16[512,512]{1,0:T(8,128)(2,1)}, bf16[512,512]{1,0:T(8,128)(2,1)}, u32[]{:S(2)}, u32[]{:S(2)}) collective-permute-start(bf16[512,512]{1,0:T(8,128)(2,1)} %collective-permute-done.1), channel_id=1, source_target_pairs={{0,8},{8,16},{16,24},{24,0},{1,9},{9,17},{17,25},{25,1},{2,10},{10... | collective-permute-start | bytes 1572872 | tf_op jit(solution)/shard_map/ppermute | solution.py:18
  77.9 13.0 %copy-start.23 = (f32[512]{0:T(512)S(1)}, f32[512]{0:T(512)}, u32[]{:S(2)}) copy-start(f32[512]{0:T(512)} %copy-done.22) | copy-start | bytes 6148
  77.9 13.0 %copy-start.30 = (f32[2048]{0:T(1024)S(1)}, f32[2048]{0:T(1024)}, u32[]{:S(2)}) copy-start(f32[2048]{0:T(1024)} %param.20) | copy-start | bytes 24580
  172.1 62.2 %collective-permute-start.3 = (bf16[2,1536]{0,1:T(8,128)(2,1)}, bf16[2,1536]{0,1:T(8,128)(2,1)}, u32[]{:S(2)}, u32[]{:S(2)}) collective-permute-start(bf16[2,1536]{0,1:T(8,128)(2,1)} %get-tuple-element.20), channel_id=1, source_target_pairs={{0,8},{8,16},{16,24},{1,9},{9,17},{17,25},{2,10},{10,18},{18,26},{... | collective-permute-start | bytes 18440 | tf_op jit(solution)/shard_map/ppermute | solution.py:31
  174.9 59.3 %collective-permute-start.4 = (bf16[2,1536]{0,1:T(8,128)(2,1)}, bf16[2,1536]{0,1:T(8,128)(2,1)}, u32[]{:S(2)}, u32[]{:S(2)}) collective-permute-start(bf16[2,1536]{0,1:T(8,128)(2,1)} %get-tuple-element.21), channel_id=1, source_target_pairs={{8,0},{16,8},{24,16},{9,1},{17,9},{25,17},{10,2},{18,10},{26,18},{... | collective-permute-start | bytes 18440 | tf_op jit(solution)/shard_map/ppermute | solution.py:33
  176.2 45.6 %copy-start.24 = (f32[512]{0:T(512)S(1)}, f32[512]{0:T(512)}, u32[]{:S(2)}) copy-start(f32[512]{0:T(512)} %copy-done.22) | copy-start | bytes 6148
  176.2 45.6 %copy-start.31 = (f32[2048]{0:T(1024)S(1)}, f32[2048]{0:T(1024)}, u32[]{:S(2)}) copy-start(f32[2048]{0:T(1024)} %param.20) | copy-start | bytes 24580
  227.3 85.7 %collective-permute-start.5 = (bf16[128,1024]{0,1:T(8,128)(2,1)}, bf16[128,1024]{0,1:T(8,128)(2,1)S(1)}, u32[]{:S(2)}, u32[]{:S(2)}) collective-permute-start(bf16[128,1024]{0,1:T(8,128)(2,1)} %get-tuple-element.37), channel_id=1, source_target_pairs={{0,8},{8,16},{16,24},{1,9},{9,17},{17,25},{2,10},{10,18},{18,26},{... | collective-permute-start | bytes 786440 | tf_op jit(solution)/shard_map/ppermute | solution.py:31
  229.3 83.7 %collective-permute-start.6 = (bf16[128,1024]{0,1:T(8,128)(2,1)}, bf16[128,1024]{0,1:T(8,128)(2,1)}, u32[]{:S(2)}, u32[]{:S(2)}) collective-permute-start(bf16[128,1024]{0,1:T(8,128)(2,1)} %get-tuple-element.38), channel_id=1, source_target_pairs={{8,0},{16,8},{24,16},{9,1},{17,9},{25,17},{10,2},{18,10},{26,18},{... | collective-permute-start | bytes 786440 | tf_op jit(solution)/shard_map/ppermute | solution.py:33
  256.6 41.5 %copy-start.8 = (f32[4,4,128,128]{3,2,1,0:T(8,128)S(1)}, f32[4,4,128,128]{3,2,1,0:T(8,128)}, u32[]{:S(2)}) copy-start(f32[4,4,128,128]{3,2,1,0:T(8,128)} %fusion.56) | copy-start | bytes 3145732
  256.6 41.5 %copy-start.18 = (f32[4,4,2,128]{3,2,1,0:T(2,128)S(1)}, f32[4,4,2,128]{3,2,1,0:T(2,128)}, u32[]{:S(2)}) copy-start(f32[4,4,2,128]{3,2,1,0:T(2,128)} %copy.184) | copy-start | bytes 49156
  490.5 14.2 %copy-start.1 = (bf16[2048,16]{0,1:T(8,128)(2,1)S(1)}, bf16[2048,16]{0,1:T(8,128)(2,1)}, u32[]{:S(2)}) copy-start(bf16[2048,16]{0,1:T(8,128)(2,1)} %param.25) | copy-start | bytes 196612
  (26 other events, 90.8 us)
Sparse Core Ops, SparseCore 0:
  8.9 64.0 all-gather.20
  74.6 46.2 all-gather.14
  122.5 44.7 all-gather.12
  168.7 53.0 all-gather.22
  223.2 58.4 all-gather.16
  283.1 80.7 all-gather.24
  365.4 79.2 all-gather.26
  446.3 44.1 all-gather.18
  496.1 8.5 reduce-scatter.1
